TPU v7x, 512 devices: a 8x2x16 block of a 8x8x16 slice. The times are simulated.
512 devices in a mesh: grp: 2 (over y), sp: 16 (over z), tp: 16 (over x, core).
Axes of the slice: x: 8, y: 2, z: 16, core: 2. Of those that a mesh axis runs over, the one named last changes fastest.
The devices are a block of a 8x8x16 slice.
Arguments:
- hidden_items: bfloat16 [4096, 4096], P(('grp', 'sp', 'tp')), parts along dimension 0, may hold values from -6 to 6
- sample_cond: bfloat16 [8192], P('grp'), parts along dimension 0, may hold values from -6 to 6
- prompt_items: bfloat16 [256, 4096], P(('grp', 'sp')), parts along dimension 0, may hold values from -6 to 6
- prompt_cond: bfloat16 [4096], replicated, may hold values from -6 to 6
- adjust_shifting: bfloat16 [4096, 4096], P('sp', 'tp'), may hold values from -0.125 to 0.125
- adjust_stretch: bfloat16 [4096, 4096], P('sp', 'tp'), may hold values from -0.125 to 0.125
- skip_valve: bfloat16 [4096, 4096], P('sp', 'tp'), may hold values from -0.125 to 0.125
- receiver_matrix: bfloat16 [4096, 2048], P(None, 'tp'), may hold values from -0.09375 to 0.09375
- address_matrix: bfloat16 [4096, 2048], P(None, 'tp'), may hold values from -0.09375 to 0.09375
- payload_matrix: bfloat16 [4096, 2048], P(None, 'tp'), may hold values from -0.09375 to 0.09375
- joint_lower_projector: bfloat16 [4096, 64], P('sp'), may hold values from -0.09375 to 0.09375
- fading_raise_matrix: bfloat16 [64, 2048], P(None, 'tp'), may hold values from -1.5 to 1.5
- step_raise_matrix: bfloat16 [64, 2048], P(None, 'tp'), may hold values from -1.5 to 1.5
- feature_fading: float32 [2048], P('tp'), may hold values from 0 to 0.1, as said below
- spike_logfade: float32 [4096, 32], P(('grp', 'sp'), 'tp'), parts along dimension 0, may hold values from 0 to 2
- group_standard_factor: float32 [2048], P('tp'), may hold values from 0.1 to 1.9
- emit_matrix: bfloat16 [2048, 4096], P('tp', 'sp'), may hold values from -0.125 to 0.125
Outputs:
- latent_out: bfloat16 [4096, 4096], P(('grp', 'sp', 'tp')), parts along dimension 0
There are 2 independent parts, one for each index of `grp`. A program takes and returns all parts, laid end to end along the dimension named above; an argument that names none is the same for every part. Nothing has to cross between parts.
Inputs may be any that keep to these rules, and one draw needn't show every extreme that they name: `feature_fading`: per-token decay rate of each channel.
All inputs are finite; a program needn't handle non-finite values.
Results may differ from a plain program's by a relative error of at most 0.015.
Values may be sent and summed in bfloat16 or wider, within the bound.
No kernel may reach another device: no remote copies, remote signals or barrier semaphores. Data moves between devices by JAX's collectives and lax.ppermute only.
A program may use at most 64 MiB of HBM per device.

v0:
```python
import math
import jax
import jax.numpy as jnp
from jax import lax
from jax.sharding import PartitionSpec as P

ATTEND_WIDTH = 64
EPS_ROW = 1e-05
EPS_HEAD = 0.00064
EPS_KEY = 1e-06
rate_shift = 5.0


def copy_for_each(shard, axis):
    peers = lax.axis_size(axis)
    return lax.all_to_all(
        jnp.broadcast_to(shard[None], (peers, *shard.shape)), axis, 0, 0, tiled=True
    )


def of_everyone(shard, axis):
    return copy_for_each(shard, axis).sum(axis=0)


def packed_total(arrays, axis):
    vector, at, gathered = (jnp.concatenate([a.reshape(-1) for a in arrays]), 0, [])
    subtotal = of_everyone(vector, axis)
    for a in arrays:
        gathered.append(subtotal[at : at + a.size].reshape(a.shape))
        at += a.size
    return tuple(gathered)


def in_one_piece(arrays, axis, dim, along):
    ends, at = ([], 0)
    for a in arrays[:-1]:
        at += a.shape[along]
        ends.append(at)
    both = jnp.concatenate(arrays, axis=along)
    return tuple(jnp.split(lax.all_gather(both, axis, axis=dim, tiled=True), ends, axis=along))


def rows_first(arrays, axis, dims):
    turned = [jnp.moveaxis(a, dim, 0) for a, dim in zip(arrays, dims)]
    both = jnp.concatenate([t.reshape(len(t), -1) for t in turned], axis=1)
    result, at, gathered = (lax.all_gather(both, axis, axis=0, tiled=True), 0, [])
    for t, dim in zip(turned, dims):
        slab = result[:, at : at + t[0].size].reshape(-1, *t.shape[1:])
        gathered.append(jnp.moveaxis(slab, 0, dim))
        at += t[0].size
    return tuple(gathered)


def collected_together(shard, axis):
    leaves = jax.tree.leaves(shard)
    order = sorted(range(len(leaves)), key=lambda k: -leaves[k].size)
    width = (1, *leaves[order[0]].shape)[-1]
    lines = [
        jnp.pad(leaves[k].reshape(-1), (0, -leaves[k].size % width)).reshape(-1, width)
        for k in order
    ]
    both, at, found = (lax.all_gather(jnp.concatenate(lines), axis), 0, {})
    for k, line in zip(order, lines):
        slab = both[:, at : at + len(line)].reshape(len(both), -1)
        found[k] = slab[:, : leaves[k].size].reshape(-1, *leaves[k].shape)
        at += len(line)
    numbers = iter(range(len(leaves)))
    return jax.tree.map(lambda _: found[next(numbers)], shard)


def entering(shard, axis, combine, identity):
    peers, mine = (lax.axis_size(axis), lax.axis_index(axis))
    everything = collected_together(
        jax.tree.map(lambda part, kind: part.astype(kind), shard, (jnp.bfloat16, jnp.bfloat16)),
        axis,
    )
    start = jax.tree.map(
        lambda part, zero: jnp.broadcast_to(jnp.asarray(zero, part.dtype), part.shape),
        shard,
        identity,
    )

    def step(k, before):
        reached = k < mine
        new = combine(
            before, jax.tree.map(lambda part, own: part[k].astype(own.dtype), everything, shard)
        )
        return jax.tree.map(lambda a, b: jnp.where(reached, a, b), new, before)

    return lax.fori_loop(0, peers, step, start)


def gathered_once(shard, axis):
    leaves = jax.tree.leaves(shard)
    order = sorted(range(len(leaves)), key=lambda k: -leaves[k].size)
    width = (1, *leaves[order[0]].shape)[-1]
    lines = [
        jnp.pad(leaves[k].reshape(-1), (0, -leaves[k].size % width)).reshape(-1, width)
        for k in order
    ]
    both, at, found = (copy_for_each(jnp.concatenate(lines), axis), 0, {})
    for k, line in zip(order, lines):
        slab = both[:, at : at + len(line)].reshape(len(both), -1)
        found[k] = slab[:, : leaves[k].size].reshape(-1, *leaves[k].shape)
        at += len(line)
    numbers = iter(range(len(leaves)))
    return jax.tree.map(lambda _: found[next(numbers)], shard)


def folded_in_pairs(pieces, combine):
    while len(jax.tree.leaves(pieces)[0]) > 1:
        pieces = jax.vmap(combine)(
            *(jax.tree.map(lambda part: part[side::2], pieces) for side in (0, 1))
        )
    return jax.tree.map(lambda part: part[0], pieces)


def entering_2(shard, axis, combine, identity):
    peers, mine = (lax.axis_size(axis), lax.axis_index(axis))
    passed = jnp.arange(peers) > mine

    def kept(part, zero, own):
        part = jnp.where(
            passed.reshape(-1, *(1 for _ in own.shape)),
            part.astype(own.dtype),
            jnp.asarray(zero, own.dtype),
        )
        return part[::-1]

    pieces = gathered_once(
        jax.tree.map(lambda part, kind: part.astype(kind), shard, (jnp.bfloat16, jnp.bfloat16)),
        axis,
    )
    return folded_in_pairs(jax.tree.map(kept, pieces, identity, shard), combine)


def cut_along(shard, dim, peers):
    dims = shard.shape
    tiles = shard.reshape(*dims[:dim], peers, dims[dim] // peers, *dims[dim + 1 :])
    return jnp.moveaxis(tiles, dim, 0)


def sent_and_summed(shard, axis, dim):
    peers = lax.axis_size(axis)
    tiles = lax.all_to_all(cut_along(shard, dim, peers), axis, 0, 0, tiled=True)
    return jnp.sum(tiles.astype(jnp.float32), axis=0)


def stored(value):
    return lax.optimization_barrier(value.astype(jnp.bfloat16))


def product(left, right):
    return jnp.dot(left, right, preferred_element_type=jnp.float32)


def batch_dot(left, right):
    return jnp.matmul(left, right)


def flipped(tensor):
    return jnp.swapaxes(tensor, -1, -2)


def modulate(rows, shifts, scales):
    values = rows.astype(jnp.float32)
    centre = jnp.mean(values, -1, keepdims=True)
    spread = jnp.mean(jnp.square(values - centre), -1, keepdims=True)
    normed = (values - centre) * lax.rsqrt(spread + EPS_ROW)
    return (normed * (1.0 + scales) + shifts).astype(jnp.bfloat16)


def both_ways(tensor):
    return jnp.stack([tensor, jnp.flip(tensor, axis=1)])


def chain_inputs(
    key_rows,
    value_rows,
    low_rows,
    query_rows,
    fading_raise_matrix,
    step_raise_matrix,
    feature_fading,
    surplus_entries,
):
    row_count = key_rows.shape[0]
    head_count = key_rows.shape[1] // ATTEND_WIDTH
    squashed = jnp.tanh(low_rows.astype(jnp.float32)).astype(jnp.bfloat16)
    logdecay = (
        -feature_fading * jax.nn.sigmoid(product(squashed, fading_raise_matrix)) - surplus_entries
    )
    learned = jax.nn.sigmoid(product(squashed, step_raise_matrix) - rate_shift)

    def by_head(tensor):
        return jnp.transpose(
            tensor.astype(jnp.float32).reshape(row_count, head_count, ATTEND_WIDTH), (1, 0, 2)
        )

    key_heads = by_head(key_rows)
    unit_keys = key_heads * lax.rsqrt(jnp.sum(key_heads * key_heads, -1, keepdims=True) + EPS_KEY)
    removal = unit_keys * by_head(learned)
    return tuple(
        (
            both_ways(tensor)
            for tensor in (
                by_head(logdecay),
                key_heads,
                by_head(value_rows),
                unit_keys,
                removal,
                by_head(query_rows),
            )
        )
    )


def sub_block(carried, inputs, reading):
    logdecay, key_heads, value_heads, unit_keys, removal, query_heads = inputs
    sub_len = logdecay.shape[-2]
    totals = jnp.cumsum(logdecay, axis=-2)
    inclusive = jnp.exp(totals)
    exclusive = jnp.exp(totals - logdecay)
    inverse = jnp.exp(-totals)
    probed = exclusive * unit_keys
    key_in = key_heads * inverse
    removal_in = removal * inverse
    places = lax.iota(jnp.int32, sub_len)
    strict = (places[:, None] > places[None, :]).astype(jnp.float32)
    system = batch_dot(probed, flipped(removal_in)) * strict + jnp.eye(sub_len, dtype=jnp.float32)
    right_side = batch_dot(probed, flipped(carried)) + batch_dot(
        batch_dot(probed, flipped(key_in)) * strict, value_heads
    )
    solved = jax.scipy.linalg.solve_triangular(system, right_side, lower=True, unit_diagonal=True)
    final_row = inclusive[..., -1:, :]
    ending = (
        carried * final_row
        + batch_dot(flipped(value_heads), key_in * final_row)
        - batch_dot(flipped(solved), removal_in * final_row)
    )
    if not reading:
        return (ending, jnp.zeros((), jnp.float32))
    weighted = inclusive * query_heads
    upto_mask = (places[:, None] >= places[None, :]).astype(jnp.float32)
    outputs = (
        batch_dot(weighted, flipped(carried))
        + batch_dot(batch_dot(weighted, flipped(key_in)) * upto_mask, value_heads)
        - batch_dot(batch_dot(weighted, flipped(removal_in)) * upto_mask, solved)
    )
    return (ending, outputs)


def run_chain(carried, inputs, reading):
    length = inputs[0].shape[-2]
    sub_len = math.gcd(64, length)

    def to_blocks(tensor):
        leading = tensor.shape[:-2]
        shaped = tensor.reshape(leading + (length // sub_len, sub_len, tensor.shape[-1]))
        return jnp.moveaxis(shaped, -3, 0)

    def advance(state_now, pieces):
        return sub_block(state_now, pieces, reading)

    ending, outputs = lax.scan(advance, carried, tuple((to_blocks(tensor) for tensor in inputs)))
    if reading:
        outputs = jnp.moveaxis(outputs, 0, -3)
        outputs = outputs.reshape(outputs.shape[:-3] + (length, outputs.shape[-1]))
    return (ending, outputs)


def shards(
    hidden_items,
    sample_cond,
    prompt_items,
    prompt_cond,
    adjust_shifting,
    adjust_stretch,
    skip_valve,
    receiver_matrix,
    address_matrix,
    payload_matrix,
    joint_lower_projector,
    fading_raise_matrix,
    step_raise_matrix,
    feature_fading,
    spike_logfade,
    group_standard_factor,
    emit_matrix,
):
    width = hidden_items.shape[1]
    span_rows = adjust_shifting.shape[0]
    conditions = jnp.stack([sample_cond, prompt_cond])
    activated = jax.nn.silu(conditions.astype(jnp.float32)).astype(jnp.bfloat16)
    own_cols = lax.dynamic_slice_in_dim(activated, lax.axis_index("sp") * span_rows, span_rows, 1)
    part_shift = product(own_cols, adjust_shifting)
    part_scale = product(own_cols, adjust_stretch)
    part_gate = product(own_cols[:1], skip_valve)
    summed = packed_total((part_shift, part_scale, part_gate), "sp")
    shifts, scales, gates = in_one_piece((summed[0], summed[1], summed[2]), "tp", 1, 0)
    out_weight, down_weight = rows_first((emit_matrix, joint_lower_projector), "sp", (1, 0))
    u_rows = modulate(hidden_items, shifts[0], scales[0])
    low_own = stored(product(u_rows, down_weight))
    joined = jnp.concatenate([u_rows, low_own], axis=1)
    portion = lax.all_gather(joined, "tp", axis=0, tiled=True)
    features = portion[:, :width]
    gathered = jnp.concatenate(
        [
            stored(product(features, receiver_matrix)),
            stored(product(features, address_matrix)),
            stored(product(features, payload_matrix)),
            portion[:, width:],
        ],
        axis=1,
    )
    head_cols = receiver_matrix.shape[1]
    head_count = head_cols // ATTEND_WIDTH
    ctx_mod = modulate(prompt_items, shifts[1], scales[1])
    ctx_keys, ctx_values, ctx_low = in_one_piece(
        (
            stored(product(ctx_mod, address_matrix)),
            stored(product(ctx_mod, payload_matrix)),
            stored(product(ctx_mod, down_weight)),
        ),
        "sp",
        0,
        1,
    )
    ctx_inputs = chain_inputs(
        ctx_keys,
        ctx_values,
        ctx_low,
        ctx_keys,
        fading_raise_matrix,
        step_raise_matrix,
        feature_fading,
        0.0,
    )
    zeroed = jnp.zeros((2, head_count, ATTEND_WIDTH, ATTEND_WIDTH), jnp.float32)
    ctx_state, _ = run_chain(zeroed, ctx_inputs, False)
    surplus_entries = jnp.repeat(spike_logfade, ATTEND_WIDTH, axis=1)
    lat_inputs = chain_inputs(
        gathered[:, head_cols : 2 * head_cols],
        gathered[:, 2 * head_cols : 3 * head_cols],
        gathered[:, 3 * head_cols :],
        gathered[:, :head_cols],
        fading_raise_matrix,
        step_raise_matrix,
        feature_fading,
        surplus_entries,
    )
    identity_maps = jnp.broadcast_to(
        jnp.eye(ATTEND_WIDTH, dtype=jnp.float32), (2, head_count, ATTEND_WIDTH, ATTEND_WIDTH)
    )
    augmented = jnp.concatenate([jnp.zeros_like(identity_maps), identity_maps], axis=2)
    padded_values = jnp.concatenate([lat_inputs[2], jnp.zeros_like(lat_inputs[2])], axis=3)
    ending, _ = run_chain(augmented, lat_inputs[:2] + (padded_values,) + lat_inputs[3:], False)
    offsets = ending[:, :, :ATTEND_WIDTH]
    factors = ending[:, :, ATTEND_WIDTH:]

    def compose(early, later):
        return (batch_dot(early[0], later[0]), batch_dot(early[1], later[0]) + later[1])

    unit_map = (identity_maps[0], jnp.zeros_like(identity_maps[0]))
    ahead = entering((factors[0], offsets[0]), "sp", compose, unit_map)
    behind = entering_2((factors[1], offsets[1]), "sp", compose, unit_map)
    starting = jnp.stack(
        [
            batch_dot(ctx_state[0], ahead[0]) + ahead[1],
            batch_dot(ctx_state[1], behind[0]) + behind[1],
        ]
    )
    _, outputs = run_chain(starting, lat_inputs, True)
    combined = outputs[0] + jnp.flip(outputs[1], axis=1)
    centre = jnp.mean(combined, -1, keepdims=True)
    spread = jnp.mean(jnp.square(combined - centre), -1, keepdims=True)
    gains = group_standard_factor.reshape(head_count, 1, ATTEND_WIDTH)
    normed = (combined - centre) * lax.rsqrt(spread + EPS_HEAD) * gains
    row_total = combined.shape[1]
    normed = jnp.transpose(normed, (1, 0, 2)).reshape(row_total, head_cols).astype(jnp.bfloat16)
    mixed_sum = sent_and_summed(product(normed, out_weight).astype(jnp.bfloat16), "tp", 0)
    return (hidden_items.astype(jnp.float32) + gates[0] * mixed_sum).astype(jnp.bfloat16)


def solution(mesh):
    placed = (
        P(("grp", "sp", "tp"), None),
        P("grp"),
        P(("grp", "sp"), None),
        P(),
        P("sp", "tp"),
        P("sp", "tp"),
        P("sp", "tp"),
        P(None, "tp"),
        P(None, "tp"),
        P(None, "tp"),
        P("sp", None),
        P(None, "tp"),
        P(None, "tp"),
        P("tp"),
        P(("grp", "sp"), "tp"),
        P("tp"),
        P("tp", "sp"),
    )
    return jax.shard_map(
        shards, mesh=mesh, in_specs=placed, out_specs=P(("grp", "sp", "tp"), None), check_vma=False
    )
```

profile of v0, /device:TPU:65, one launch (start us, length us, event | category | flops | bytes accessed | tf_op | source)
XLA Modules:
  0.0 458.1 jit_solution(16582487184394105169)
XLA Ops:
  8.2 1.0 fusion.132
  9.2 1.1 convolution_bitcast_fusion.3
  10.4 1.1 convolution_bitcast_fusion.4
  12.1 44.2 %all-to-all-start = ((f32[16,1,1280]{2,1,0:T(1,128)}), f32[16,1,1280]{2,1,0:T(1,128)S(1)}, u32[]{:S(2)}, u32[]{:S(2)}) async-start(f32[16,1,1280]{2,1,0:T(1,128)} %broadcast_in_dim.39), calls=%async_computation | async-start | bytes 163840 | tf_op jit(solution)/shard_map/all_to_all | solution.py:16
  56.4 1.5 pad_maximum_fusion.2
  60.3 7.6 %all-to-all-done = f32[16,1,1280]{2,1,0:T(1,128)S(1)} async-done(((f32[16,1,1280]{2,1,0:T(1,128)}), f32[16,1,1280]{2,1,0:T(1,128)S(1)}, u32[]{:S(2)}, u32[]{:S(2)}) %all-to-all-start) | async-done | bytes 81952 | tf_op jit(solution)/shard_map/all_to_all | solution.py:16
  68.0 20.4 %all_gather.18 = f32[5,4096]{1,0:T(8,128)S(1)} all-gather(f32[5,256]{1,0:T(8,128)S(1)} %pad_maximum_fusion.7), channel_id=1, replica_groups=mesh['grp'=2,'sp'=16,'tp'=16] {'tp'}, dimensions={1}, use_global_device_ids=true | all-gather | bytes 87040 | tf_op jit(solution)/shard_map/all_gather | solution.py:40
  89.3 38.7 %all-gather.4.cloned.1.call-done = bf16[4096,192]{0,1:T(8,128)(2,1)} async-done(((bf16[256,192]{0,1:T(8,128)(2,1)}), bf16[4096,192]{0,1:T(8,128)(2,1)}) %all-gather.4.cloned.1.call-update) | async-done | bytes 1572880 | tf_op jit(solution)/shard_map/all_gather | solution.py:46
  128.0 1.3 convolution_convert_fusion.5
  129.3 21.7 %all_gather.20 = bf16[128,320]{1,0:T(8,128)(2,1)S(1)} all-gather(bf16[8,320]{1,0:T(8,128)(2,1)S(1)} %pad_maximum_fusion.8), channel_id=1, replica_groups=mesh['grp'=2,'sp'=16,'tp'=16] {'sp'}, dimensions={0}, use_global_device_ids=true | all-gather | bytes 87040 | tf_op jit(solution)/shard_map/all_gather | solution.py:40
  152.9 1.3 convolution_convert_fusion.4
  155.7 1.0 maximum_bitcast_fusion
  157.0 46.8 %while.51 = (s32[]{:T(128)}, f32[2,2,64,64]{3,2,1,0:T(8,128)S(1)}, f32[2,2,2,64,64]{3,0,4,2,1:T(2,128)}, f32[2,2,2,64,64]{3,0,4,2,1:T(2,128)S(1)}, f32[2,2,2,64,...) while((s32[]{:T(128)}, f32[2,2,64,64]{3,2,1,0:T(8,128)S(1)}, ...), condition=%wide.region_6.8_spmd.clone, body=%wide.region_4.7_spmd.clone.sunk | while | flops 26669124 | bytes 3338888 | solution.py:265
  157.3 1.1 constant_dynamic-slice_fusion.16
  160.1 19.7 %custom-call.18 = f32[2,2,1,64,64]{3,4,2,1,0:T(8,128)S(1)} custom-call(f32[2,2,1,64,64]{4,3,2,1,0:T(8,128)S(1)} %fusion.288), custom_call_target="InvertDiagBlocksLowerTriangular" | custom-call | tf_op jit(solution)/shard_map/while/body/eval_jaxpr/jit(_solve_triangular)/vmap(vmap())/triangular_solve | solution.py:234
  180.7 1.1 constant_dynamic-slice_fusion.16
  183.5 19.7 %custom-call.18 = f32[2,2,1,64,64]{3,4,2,1,0:T(8,128)S(1)} custom-call(f32[2,2,1,64,64]{4,3,2,1,0:T(8,128)S(1)} %fusion.288), custom_call_target="InvertDiagBlocksLowerTriangular" | custom-call | tf_op jit(solution)/shard_map/while/body/eval_jaxpr/jit(_solve_triangular)/vmap(vmap())/triangular_solve | solution.py:234
  203.8 10.1 %all-gather.6.cloned.1.call-done = bf16[128,4160]{1,0:T(8,128)(2,1)} async-done(((bf16[8,4160]{1,0:T(8,128)(2,1)}), bf16[128,4160]{1,0:T(8,128)(2,1)}) %all-gather.6.cloned.1.call-update) | async-done | bytes 1064976 | tf_op jit(solution)/shard_map/all_gather | solution.py:305
  213.9 1.0 fusion.83
  215.2 1.7 convolution_convert_fusion.2
  217.2 1.0 fusion.78
  220.3 1.6 convolution_convert_fusion.3
  224.1 42.9 %while.49 = (s32[]{:T(128)}, f32[2,2,128,64]{2,3,1,0:T(8,128)S(1)}, f32[2,2,2,64,64]{4,3,2,1,0:T(8,128)S(1)}, bf16[2,2,2,64,128]{4,3,0,2,1:T(8,128)(2,1)S(1)}, f...) while((s32[]{:T(128)}, f32[2,2,128,64]{2,3,1,0:T(8,128)S(1)}, ...), condition=%wide.region_12.14_spmd, body=%wide.region_10.13_spmd.sunk | while | flops 47673408 | bytes 4268149 | solution.py:265
  225.3 19.7 %custom-call.16 = f32[2,2,1,64,64]{3,4,2,1,0:T(8,128)S(1)} custom-call(f32[2,2,1,64,64]{4,3,2,1,0:T(8,128)S(1)} %fusion.251), custom_call_target="InvertDiagBlocksLowerTriangular" | custom-call | tf_op jit(solution)/shard_map/while/body/eval_jaxpr/jit(_solve_triangular)/vmap(vmap())/triangular_solve | solution.py:234
  246.7 19.7 %custom-call.16 = f32[2,2,1,64,64]{3,4,2,1,0:T(8,128)S(1)} custom-call(f32[2,2,1,64,64]{4,3,2,1,0:T(8,128)S(1)} %fusion.251), custom_call_target="InvertDiagBlocksLowerTriangular" | custom-call | tf_op jit(solution)/shard_map/while/body/eval_jaxpr/jit(_solve_triangular)/vmap(vmap())/triangular_solve | solution.py:234
  267.4 0.8 broadcast_in_dim.44
  268.3 12.5 %all-to-all-start.1 = ((bf16[16,256,64]{1,2,0:T(8,128)(2,1)}), bf16[16,256,64]{1,2,0:T(8,128)(2,1)S(1)}, u32[]{:S(2)}, u32[]{:S(2)}) async-start(bf16[16,256,64]{1,2,0:T(8,128)(2,1)} %broadcast_in_dim.44), calls=%async_computation.1 | async-start | bytes 1048576 | tf_op jit(solution)/shard_map/all_to_all | solution.py:16
  281.1 45.0 %all-gather = bf16[4096,64]{0,1:T(8,128)(2,1)S(1)} all-gather(bf16[256,64]{0,1:T(8,128)(2,1)S(1)} %pad_maximum_fusion.4), channel_id=2, replica_groups=mesh['grp'=2,'sp'=16,'tp'=16] {'sp'}, dimensions={0}, use_global_device_ids=true | all-gather | bytes 557056 | tf_op jit(solution)/shard_map/all_gather | solution.py:62
  326.4 1.1 reshape_reshape.8
  327.5 1.1 reshape_reshape.9
  328.6 18.0 %while.52 = (s32[]{:T(128)}, bf16[2,64,64]{1,2,0:T(8,128)(2,1)S(1)}, f32[2,64,64]{1,2,0:T(8,128)S(1)}, s32[]{:T(128)}, bf16[16,2,64,64]{2,1,3,0:T(2,128)(2,1)}, ...) while((s32[]{:T(128)}, bf16[2,64,64]{1,2,0:T(8,128)(2,1)S(1)}, ...), condition=%wide.region_14.16_spmd.clone, body=%wide.region_13.15_spmd.clone.sunk | while | flops 2146308 | bytes 311414 | solution.py:90
  328.7 0.8 constant_dynamic-slice_fusion.18
  329.8 0.8 constant_dynamic-slice_fusion.18
  330.9 0.8 constant_dynamic-slice_fusion.18
  332.0 0.8 constant_dynamic-slice_fusion.18
  333.2 0.8 constant_dynamic-slice_fusion.18
  335.4 0.8 constant_dynamic-slice_fusion.18
  346.9 2.0 convolution_convert_fusion.1
  350.2 1.1 maximum_bitcast_fusion.9
  351.3 1.0 fusion.140
  352.3 1.4 copy.217
  358.2 49.5 %while.50 = (s32[]{:T(128)}, f32[2,2,64,64]{3,2,1,0:T(8,128)S(1)}, f32[2,2,2,64,64]{4,3,2,1,0:T(8,128)}, f32[2,2,2,64,64]{4,3,2,1,0:T(8,128)S(1)}, f32[2,2,2,64,...) while((s32[]{:T(128)}, f32[2,2,64,64]{3,2,1,0:T(8,128)S(1)}, ...), condition=%wide.region_17.19_spmd, body=%wide.region_15.18_spmd.sunk | while | flops 37163072 | bytes 5173957 | solution.py:265
  358.2 1.3 constant_dynamic-slice_fusion.14
  360.9 19.7 %custom-call.17 = f32[2,2,1,64,64]{3,4,2,1,0:T(8,128)S(1)} custom-call(f32[2,2,1,64,64]{4,3,2,1,0:T(8,128)S(1)} %fusion.273), custom_call_target="InvertDiagBlocksLowerTriangular" | custom-call | tf_op jit(solution)/shard_map/while/body/eval_jaxpr/jit(_solve_triangular)/vmap(vmap())/triangular_solve | solution.py:234
  383.0 1.3 constant_dynamic-slice_fusion.14
  385.7 19.7 %custom-call.17 = f32[2,2,1,64,64]{3,4,2,1,0:T(8,128)S(1)} custom-call(f32[2,2,1,64,64]{4,3,2,1,0:T(8,128)S(1)} %fusion.273), custom_call_target="InvertDiagBlocksLowerTriangular" | custom-call | tf_op jit(solution)/shard_map/while/body/eval_jaxpr/jit(_solve_triangular)/vmap(vmap())/triangular_solve | solution.py:234
  407.7 1.1 fusion.141
  410.0 39.7 %all_to_all.16 = bf16[16,8,4096]{2,1,0:T(8,128)(2,1)S(1)} all-to-all(bf16[16,8,4096]{2,1,0:T(8,128)(2,1)S(1)} %fusion.70), channel_id=1, replica_groups=mesh['grp'=2,'sp'=16,'tp'=16] {'tp'}, dimensions={0} | all-to-all | bytes 2097152 | tf_op jit(solution)/shard_map/all_to_all | solution.py:145
  (386 shorter events, 51.7 us)
Async XLA Ops:
  6.5 82.3 %copy-start = (bf16[4096,128]{1,0:T(8,128)(2,1)S(1)}, bf16[4096,128]{1,0:T(8,128)(2,1)}, u32[]{:S(2)}) copy-start(bf16[4096,128]{1,0:T(8,128)(2,1)} %param.35) | copy-start | bytes 3145732
  6.6 51.5 %copy-start.3 = (bf16[8,4096]{1,0:T(8,128)(2,1)S(1)}, bf16[8,4096]{1,0:T(8,128)(2,1)}, u32[]{:S(2)}) copy-start(bf16[8,4096]{1,0:T(8,128)(2,1)} %param.27) | copy-start | bytes 196612
  6.6 51.9 %copy-start.7 = (bf16[8,4096]{1,0:T(8,128)(2,1)S(1)}, bf16[8,4096]{1,0:T(8,128)(2,1)}, u32[]{:S(2)}) copy-start(bf16[8,4096]{1,0:T(8,128)(2,1)} %param.29) | copy-start | bytes 196612
  6.6 53.0 %copy-start.27 = (f32[128]{0:T(128)S(1)}, f32[128]{0:T(128)}, u32[]{:S(2)}) copy-start(f32[128]{0:T(128)} %param.40) | copy-start | bytes 1540
  6.6 53.0 %copy-start.28 = (f32[128]{0:T(128)S(1)}, f32[128]{0:T(128)}, u32[]{:S(2)}) copy-start(f32[128]{0:T(128)} %param.42) | copy-start | bytes 1540
  9.2 79.3 %copy-start.5 = (bf16[4096,128]{1,0:T(8,128)(2,1)S(1)}, bf16[4096,128]{1,0:T(8,128)(2,1)}, u32[]{:S(2)}) copy-start(bf16[4096,128]{1,0:T(8,128)(2,1)} %param.36) | copy-start | bytes 3145732
  12.1 55.8 %all-to-all-start = ((f32[16,1,1280]{2,1,0:T(1,128)}), f32[16,1,1280]{2,1,0:T(1,128)S(1)}, u32[]{:S(2)}, u32[]{:S(2)}) async-start(f32[16,1,1280]{2,1,0:T(1,128)} %broadcast_in_dim.39), calls=%async_computation | async-start | bytes 163840 | tf_op jit(solution)/shard_map/all_to_all | solution.py:16
  56.3 71.6 %all-gather.4.cloned.1.call-start = ((), (), s32[]{:S(2)}) async-start(), calls=%async_computation.3 | async-start | bytes 1671168 | tf_op jit(solution)/shard_map/all_gather | solution.py:46
  58.0 155.9 %all-gather.6.cloned.1.call-start = ((), (), s32[]{:S(2)}) async-start(), calls=%async_computation.4 | async-start | bytes 1148928 | tf_op jit(solution)/shard_map/all_gather | solution.py:305
  58.1 2.1 copy-start.11
  59.5 0.7 copy-start.13
  88.9 62.2 %copy-start.24 = (bf16[64,128]{1,0:T(8,128)(2,1)S(1)}, bf16[64,128]{1,0:T(8,128)(2,1)}, u32[]{:S(2)}) copy-start(bf16[64,128]{1,0:T(8,128)(2,1)} %param.38) | copy-start | bytes 49156
  129.3 22.9 %copy-start.25 = (bf16[64,128]{1,0:T(8,128)(2,1)S(1)}, bf16[64,128]{1,0:T(8,128)(2,1)}, u32[]{:S(2)}) copy-start(bf16[64,128]{1,0:T(8,128)(2,1)} %param.39) | copy-start | bytes 49156
  157.0 56.9 %copy-start.22 = (f32[128,2]{0,1:T(2,128)S(1)}, f32[128,2]{0,1:T(2,128)}, u32[]{:S(2)}) copy-start(f32[128,2]{0,1:T(2,128)} %param.41) | copy-start | bytes 3076
  215.1 2.0 copy-start.26
  218.2 2.2 copy-start.6
  222.0 1.1 copy-start.16
  222.2 0.6 copy-start.8
  222.8 0.8 copy-start.15
  268.3 83.0 %all-to-all-start.1 = ((bf16[16,256,64]{1,2,0:T(8,128)(2,1)}), bf16[16,256,64]{1,2,0:T(8,128)(2,1)S(1)}, u32[]{:S(2)}, u32[]{:S(2)}) async-start(bf16[16,256,64]{1,2,0:T(8,128)(2,1)} %broadcast_in_dim.44), calls=%async_computation.1 | async-start | bytes 1048576 | tf_op jit(solution)/shard_map/all_to_all | solution.py:16
  326.4 2.2 copy-start.14
  328.6 18.1 %copy-start.9 = (f32[2,128,64]{1,2,0:T(8,128)S(1)}, f32[2,128,64]{1,2,0:T(8,128)}, u32[]{:S(2)}) copy-start(f32[2,128,64]{1,2,0:T(8,128)} %copy-done.8) | copy-start | bytes 196612
  352.3 1.4 copy-start.21
  353.9 1.6 copy-start.2
  353.9 1.9 copy-start.12
  356.0 1.0 copy-start.10
  356.0 1.1 copy-start.19
  357.3 0.9 copy-start.20
  381.0 1.0 copy-start.17
  382.2 0.7 copy-start.18
  405.7 1.0 copy-start.17
  407.0 0.7 copy-start.18
  407.7 1.8 copy-start.23
  407.7 1.9 copy-start.1
  449.8 0.8 copy-start.4
Sparse Core Ops, SparseCore 0:
  59.2 68.7 all-gather.3
  155.0 58.8 all-gather.5
where the time goes:
time: 460 us; the launch traced here: 458 us
  other arithmetic  129 us (28%)
  blocking collectives  127 us (28%)
  starting transfers between devices  56.9 us (12%)
  waiting for transfers between devices  56.5 us (12%)
  local copies, waits for them, and re-layouts  42.8 us (9%)
  matrix products  30.6 us (7%)
  between operations  14.5 us (3%)
    another operation x18, other arithmetic, sub_block(): jax.scipy.linalg.solve_triangular(system, right_side, lower=True, unit_di...  119 us
    all_to_all x2, starting transfers between devices, copy_for_each(): lax.all_to_all(jnp.broadcast_to(shard[None], (peers, *shard.shape)), axis...  56.7 us
    all_gather x1, blocking collectives, collected_together(): both, at, found = (lax.all_gather(jnp.concatenate(lines), axis), 0, {})  45 us
    all_gather x2, blocking collectives, in_one_piece(): lax.all_gather(both, axis, axis=dim, tiled=True)  42.1 us
    all_to_all x1, blocking collectives, sent_and_summed(): tiles = lax.all_to_all(cut_along(shard, dim, peers), axis, 0, 0, tiled=True)  39.7 us
    all_gather x1, waiting for transfers between devices, rows_first(): lax.all_gather(both, axis, axis=0, tiled=True)  38.7 us
    dot_general x15, matrix products, product(): return jnp.dot(left, right, preferred_element_type=jnp.float32)  14.6 us
    dot_general x77, matrix products, batch_dot(): return jnp.matmul(left, right)  13.7 us
  transfers between devices with their start and end apart: 4, of which 3 were waited for; matrix products, arithmetic and copies ran while one was open for 17% of the time, Pallas kernels for 0%

commit v1 on v0

--- a/solution.py
+++ b/solution.py
@@ -43,7 +43,13 @@
 def rows_first(arrays, axis, dims):
     turned = [jnp.moveaxis(a, dim, 0) for a, dim in zip(arrays, dims)]
     both = jnp.concatenate([t.reshape(len(t), -1) for t in turned], axis=1)
-    result, at, gathered = (lax.all_gather(both, axis, axis=0, tiled=True), 0, [])
+    result, at, gathered = (
+        jnp.concatenate(
+            lax.all_to_all(jnp.stack([both for _ in range(lax.axis_size(axis))]), axis, 0, 0), 0
+        ),
+        0,
+        [],
+    )
     for t, dim in zip(turned, dims):
         slab = result[:, at : at + t[0].size].reshape(-1, *t.shape[1:])
         gathered.append(jnp.moveaxis(slab, 0, dim))

time: 460 us -> 476 us (1.035)
  local copies, waits for them, and re-layouts: 42.8 us -> 52.5 us
    all_to_all x0 -> x1, waiting for transfers between devices: none -> 44.5 us  [rows_first(): lax.all_to_all(jnp.stack([both for _ in range(lax.axis_size(axis))]), axi...]
    all_gather x1 -> x0, waiting for transfers between devices: 38.7 us -> none  [rows_first(): lax.all_gather(both, axis, axis=0, tiled=True)]
    all_gather x1, waiting for transfers between devices: 10.1 us -> 0.46 us  [shards(): portion = lax.all_gather(joined, 'tp', axis=0, tiled=True)]
    another operation x22, local copies, waits for them, and re-layouts: 2.9 us -> 8.36 us  [both_ways(): return jnp.stack([tensor, jnp.flip(tensor, axis=1)])]
where the time goes in v1:
time: 476 us; the launch traced here: 473 us
  other arithmetic  128 us (27%)
  blocking collectives  128 us (27%)
  starting transfers between devices  61.6 us (13%)
  waiting for transfers between devices  55.7 us (12%)
  local copies, waits for them, and re-layouts  52.5 us (11%)
  matrix products  31 us (7%)
  between operations  14.5 us (3%)
    another operation x18, other arithmetic, sub_block(): jax.scipy.linalg.solve_triangular(system, right_side, lower=True, unit_di...  119 us
    all_to_all x2, starting transfers between devices, copy_for_each(): lax.all_to_all(jnp.broadcast_to(shard[None], (peers, *shard.shape)), axis...  56.9 us
    all_gather x1, blocking collectives, collected_together(): both, at, found = (lax.all_gather(jnp.concatenate(lines), axis), 0, {})  44.9 us
    all_to_all x1, waiting for transfers between devices, rows_first(): lax.all_to_all(jnp.stack([both for _ in range(lax.axis_size(axis))]), axi...  44.5 us
    all_gather x2, blocking collectives, in_one_piece(): lax.all_gather(both, axis, axis=dim, tiled=True)  43.4 us
    all_to_all x1, blocking collectives, sent_and_summed(): tiles = lax.all_to_all(cut_along(shard, dim, peers), axis, 0, 0, tiled=True)  40.1 us
    dot_general x77, matrix products, batch_dot(): return jnp.matmul(left, right)  15 us
    dot_general x15, matrix products, product(): return jnp.dot(left, right, preferred_element_type=jnp.float32)  13.6 us
  transfers between devices with their start and end apart: 4, of which 3 were waited for; matrix products, arithmetic and copies ran while one was open for 17% of the time, Pallas kernels for 0%

profile of v1, /device:TPU:65, one launch (start us, length us, event | category | flops | bytes accessed | tf_op | source)
XLA Modules:
  0.0 473.1 jit_solution(10789169859672827436)
XLA Ops:
  8.1 1.0 fusion.132
  9.2 1.1 convolution_bitcast_fusion.3
  10.2 1.1 convolution_bitcast_fusion.4
  12.0 44.2 %all-to-all-start = ((f32[16,1,1280]{2,1,0:T(1,128)}), f32[16,1,1280]{2,1,0:T(1,128)S(1)}, u32[]{:S(2)}, u32[]{:S(2)}) async-start(f32[16,1,1280]{2,1,0:T(1,128)} %broadcast_in_dim.39), calls=%async_computation | async-start | bytes 163840 | tf_op jit(solution)/shard_map/all_to_all | solution.py:16
  57.1 10.7 %all-to-all-done = f32[16,1,1280]{2,1,0:T(1,128)S(1)} async-done(((f32[16,1,1280]{2,1,0:T(1,128)}), f32[16,1,1280]{2,1,0:T(1,128)S(1)}, u32[]{:S(2)}, u32[]{:S(2)}) %all-to-all-start) | async-done | bytes 81952 | tf_op jit(solution)/shard_map/all_to_all | solution.py:16
  67.8 1.4 stack.145
  69.2 4.6 all-to-all-start.1
  76.3 20.1 %all_gather.15 = f32[5,4096]{1,0:T(8,128)S(1)} all-gather(f32[5,256]{1,0:T(8,128)S(1)} %pad_maximum_fusion.7), channel_id=1, replica_groups=mesh['grp'=2,'sp'=16,'tp'=16] {'tp'}, dimensions={1}, use_global_device_ids=true | all-gather | bytes 87040 | tf_op jit(solution)/shard_map/all_gather | solution.py:40
  96.4 1.5 convolution_convert_fusion.6
  98.4 44.5 %all-to-all-done.1 = bf16[16,256,192]{1,2,0:T(8,128)(2,1)S(1)} async-done(((bf16[16,256,192]{1,2,0:T(8,128)(2,1)}), bf16[16,256,192]{1,2,0:T(8,128)(2,1)S(1)}, u32[]{:S(2)}, u32[]{:S(2)}) %all-to-all-start.1) | async-done | bytes 1572896 | tf_op jit(solution)/shard_map/all_to_all | solution.py:48
  142.9 1.2 copy-done.3
  144.1 1.6 copy.312
  146.0 23.3 %all_gather.16 = bf16[128,320]{1,0:T(8,128)(2,1)S(1)} all-gather(bf16[8,320]{1,0:T(8,128)(2,1)S(1)} %pad_maximum_fusion.8), channel_id=1, replica_groups=mesh['grp'=2,'sp'=16,'tp'=16] {'sp'}, dimensions={0}, use_global_device_ids=true | all-gather | bytes 87040 | tf_op jit(solution)/shard_map/all_gather | solution.py:40
  176.7 1.0 stack.147
  177.6 1.0 stack.150
  178.6 1.0 stack.153
  179.6 1.0 stack.156
  180.5 1.0 stack.159
  181.7 1.0 maximum_bitcast_fusion
  183.0 46.8 %while.51 = (s32[]{:T(128)}, f32[2,2,64,64]{3,2,1,0:T(8,128)S(1)}, f32[2,2,2,64,64]{3,0,4,2,1:T(2,128)}, f32[2,2,2,64,64]{3,0,4,2,1:T(2,128)S(1)}, f32[2,2,2,64,...) while((s32[]{:T(128)}, f32[2,2,64,64]{3,2,1,0:T(8,128)S(1)}, ...), condition=%wide.region_6.8_spmd.clone, body=%wide.region_4.7_spmd.clone.sunk | while | flops 26669124 | bytes 3338888 | solution.py:271
  183.3 1.1 constant_dynamic-slice_fusion.16
  186.1 19.7 %custom-call.18 = f32[2,2,1,64,64]{3,4,2,1,0:T(8,128)S(1)} custom-call(f32[2,2,1,64,64]{4,3,2,1,0:T(8,128)S(1)} %fusion.288), custom_call_target="InvertDiagBlocksLowerTriangular" | custom-call | tf_op jit(solution)/shard_map/while/body/eval_jaxpr/jit(_solve_triangular)/vmap(vmap())/triangular_solve | solution.py:240
  206.6 1.1 constant_dynamic-slice_fusion.16
  209.5 19.7 %custom-call.18 = f32[2,2,1,64,64]{3,4,2,1,0:T(8,128)S(1)} custom-call(f32[2,2,1,64,64]{4,3,2,1,0:T(8,128)S(1)} %fusion.288), custom_call_target="InvertDiagBlocksLowerTriangular" | custom-call | tf_op jit(solution)/shard_map/while/body/eval_jaxpr/jit(_solve_triangular)/vmap(vmap())/triangular_solve | solution.py:240
  230.2 1.0 fusion.83
  231.4 1.6 convolution_convert_fusion.2
  233.5 1.0 fusion.78
  236.6 1.6 convolution_convert_fusion.3
  240.3 42.9 %while.49 = (s32[]{:T(128)}, f32[2,2,128,64]{2,3,1,0:T(8,128)S(1)}, f32[2,2,2,64,64]{4,3,2,1,0:T(8,128)S(1)}, bf16[2,2,2,64,128]{4,3,0,2,1:T(8,128)(2,1)S(1)}, f...) while((s32[]{:T(128)}, f32[2,2,128,64]{2,3,1,0:T(8,128)S(1)}, ...), condition=%wide.region_12.14_spmd, body=%wide.region_10.13_spmd.sunk | while | flops 47673408 | bytes 4268149 | solution.py:271
  241.4 19.7 %custom-call.16 = f32[2,2,1,64,64]{3,4,2,1,0:T(8,128)S(1)} custom-call(f32[2,2,1,64,64]{4,3,2,1,0:T(8,128)S(1)} %fusion.251), custom_call_target="InvertDiagBlocksLowerTriangular" | custom-call | tf_op jit(solution)/shard_map/while/body/eval_jaxpr/jit(_solve_triangular)/vmap(vmap())/triangular_solve | solution.py:240
  262.9 19.7 %custom-call.16 = f32[2,2,1,64,64]{3,4,2,1,0:T(8,128)S(1)} custom-call(f32[2,2,1,64,64]{4,3,2,1,0:T(8,128)S(1)} %fusion.251), custom_call_target="InvertDiagBlocksLowerTriangular" | custom-call | tf_op jit(solution)/shard_map/while/body/eval_jaxpr/jit(_solve_triangular)/vmap(vmap())/triangular_solve | solution.py:240
  284.5 12.7 %all-to-all-start.2 = ((bf16[16,256,64]{1,2,0:T(8,128)(2,1)}), bf16[16,256,64]{1,2,0:T(8,128)(2,1)S(1)}, u32[]{:S(2)}, u32[]{:S(2)}) async-start(bf16[16,256,64]{1,2,0:T(8,128)(2,1)} %broadcast_in_dim.44), calls=%async_computation.2 | async-start | bytes 1048576 | tf_op jit(solution)/shard_map/all_to_all | solution.py:16
  297.5 44.9 %all-gather = bf16[4096,64]{0,1:T(8,128)(2,1)S(1)} all-gather(bf16[256,64]{0,1:T(8,128)(2,1)S(1)} %pad_maximum_fusion.4), channel_id=2, replica_groups=mesh['grp'=2,'sp'=16,'tp'=16] {'sp'}, dimensions={0}, use_global_device_ids=true | all-gather | bytes 557056 | tf_op jit(solution)/shard_map/all_gather | solution.py:68
  342.7 1.1 reshape_reshape.8
  343.8 1.0 reshape_reshape.9
  344.9 18.0 %while.52 = (s32[]{:T(128)}, bf16[2,64,64]{1,2,0:T(8,128)(2,1)S(1)}, f32[2,64,64]{1,2,0:T(8,128)S(1)}, s32[]{:T(128)}, bf16[16,2,64,64]{2,1,3,0:T(2,128)(2,1)}, ...) while((s32[]{:T(128)}, bf16[2,64,64]{1,2,0:T(8,128)(2,1)S(1)}, ...), condition=%wide.region_14.16_spmd.clone, body=%wide.region_13.15_spmd.clone.sunk | while | flops 2146308 | bytes 311414 | solution.py:96
  363.2 2.0 convolution_convert_fusion.1
  366.5 1.1 maximum_bitcast_fusion.9
  367.6 1.0 fusion.140
  368.6 1.4 copy.272
  374.5 48.5 %while.50 = (s32[]{:T(128)}, f32[2,2,64,64]{3,2,1,0:T(8,128)S(1)}, f32[2,2,2,64,64]{4,3,2,1,0:T(8,128)}, f32[2,2,2,64,64]{4,3,2,1,0:T(8,128)S(1)}, f32[2,2,2,64,...) while((s32[]{:T(128)}, f32[2,2,64,64]{3,2,1,0:T(8,128)S(1)}, ...), condition=%wide.region_17.19_spmd, body=%wide.region_15.18_spmd.sunk | while | flops 37163072 | bytes 3814029 | solution.py:271
  374.5 1.3 constant_dynamic-slice_fusion.14
  377.2 19.7 %custom-call.17 = f32[2,2,1,64,64]{3,4,2,1,0:T(8,128)S(1)} custom-call(f32[2,2,1,64,64]{4,3,2,1,0:T(8,128)S(1)} %fusion.273), custom_call_target="InvertDiagBlocksLowerTriangular" | custom-call | tf_op jit(solution)/shard_map/while/body/eval_jaxpr/jit(_solve_triangular)/vmap(vmap())/triangular_solve | solution.py:240
  397.8 1.0 fusion.277
  398.7 1.3 constant_dynamic-slice_fusion.14
  401.4 19.7 %custom-call.17 = f32[2,2,1,64,64]{3,4,2,1,0:T(8,128)S(1)} custom-call(f32[2,2,1,64,64]{4,3,2,1,0:T(8,128)S(1)} %fusion.273), custom_call_target="InvertDiagBlocksLowerTriangular" | custom-call | tf_op jit(solution)/shard_map/while/body/eval_jaxpr/jit(_solve_triangular)/vmap(vmap())/triangular_solve | solution.py:240
  423.0 1.1 fusion.141
  425.3 40.1 %all_to_all.21 = bf16[16,8,4096]{2,1,0:T(8,128)(2,1)S(1)} all-to-all(bf16[16,8,4096]{2,1,0:T(8,128)(2,1)S(1)} %fusion.70), channel_id=1, replica_groups=mesh['grp'=2,'sp'=16,'tp'=16] {'tp'}, dimensions={0} | all-to-all | bytes 2097152 | tf_op jit(solution)/shard_map/all_to_all | solution.py:151
  (389 shorter events, 60.0 us)
Async XLA Ops:
  6.5 91.4 %copy-start = (bf16[4096,128]{1,0:T(8,128)(2,1)S(1)}, bf16[4096,128]{1,0:T(8,128)(2,1)}, u32[]{:S(2)}) copy-start(bf16[4096,128]{1,0:T(8,128)(2,1)} %param.35) | copy-start | bytes 3145732
  12.0 55.8 %all-to-all-start = ((f32[16,1,1280]{2,1,0:T(1,128)}), f32[16,1,1280]{2,1,0:T(1,128)S(1)}, u32[]{:S(2)}, u32[]{:S(2)}) async-start(f32[16,1,1280]{2,1,0:T(1,128)} %broadcast_in_dim.39), calls=%async_computation | async-start | bytes 163840 | tf_op jit(solution)/shard_map/all_to_all | solution.py:16
  69.2 4.8 %copy-start.28 = (f32[128]{0:T(128)S(1)}, f32[128]{0:T(128)}, u32[]{:S(2)}) copy-start(f32[128]{0:T(128)} %param.40) | copy-start | bytes 1540
  69.2 4.9 %copy-start.29 = (f32[128]{0:T(128)S(1)}, f32[128]{0:T(128)}, u32[]{:S(2)}) copy-start(f32[128]{0:T(128)} %param.42) | copy-start | bytes 1540
  69.2 6.2 %copy-start.5 = (bf16[8,4096]{1,0:T(8,128)(2,1)S(1)}, bf16[8,4096]{1,0:T(8,128)(2,1)}, u32[]{:S(2)}) copy-start(bf16[8,4096]{1,0:T(8,128)(2,1)} %param.27) | copy-start | bytes 196612
  69.2 6.4 %copy-start.8 = (bf16[8,4096]{1,0:T(8,128)(2,1)S(1)}, bf16[8,4096]{1,0:T(8,128)(2,1)}, u32[]{:S(2)}) copy-start(bf16[8,4096]{1,0:T(8,128)(2,1)} %param.29) | copy-start | bytes 196612
  69.2 73.7 %all-to-all-start.1 = ((bf16[16,256,192]{1,2,0:T(8,128)(2,1)}), bf16[16,256,192]{1,2,0:T(8,128)(2,1)S(1)}, u32[]{:S(2)}, u32[]{:S(2)}) async-start(bf16[16,256,192]{1,2,0:T(8,128)(2,1)} %stack.145), calls=%async_computation.1 | async-start | bytes 3145728 | tf_op jit(solution)/shard_map/all_to_all | solution.py:48
  73.8 156.4 %all-gather.3.cloned.1.call-start = ((), (), s32[]{:S(2)}) async-start(), calls=%async_computation.4 | async-start | bytes 1148928 | tf_op jit(solution)/shard_map/all_gather | solution.py:311
  73.9 0.8 copy-start.14
  74.0 0.7 copy-start.16
  74.0 95.3 %copy-start.30 = (f32[128]{0:T(128)}, f32[128]{0:T(128)S(1)}, u32[]{:S(2)}) copy-start(f32[128]{0:T(128)S(1)} %neg.30) | copy-start | bytes 1540
  142.9 1.2 copy-start.3
  144.1 25.3 %copy-start.25 = (bf16[64,128]{1,0:T(8,128)(2,1)S(1)}, bf16[64,128]{1,0:T(8,128)(2,1)}, u32[]{:S(2)}) copy-start(bf16[64,128]{1,0:T(8,128)(2,1)} %param.38) | copy-start | bytes 49156
  145.7 30.0 %copy-start.1 = (bf16[16,24,8,256]{3,2,0,1:T(8,128)(2,1)}, bf16[16,24,8,256]{3,2,0,1:T(8,128)(2,1)S(1)}, u32[]{:S(2)}) copy-start(bf16[16,24,8,256]{3,2,0,1:T(8,128)(2,1)S(1)} %copy.312) | copy-start | bytes 4718596
  145.7 27.3 %copy-start.26 = (bf16[64,128]{1,0:T(8,128)(2,1)S(1)}, bf16[64,128]{1,0:T(8,128)(2,1)}, u32[]{:S(2)}) copy-start(bf16[64,128]{1,0:T(8,128)(2,1)} %param.39) | copy-start | bytes 49156
  175.7 7.0 %copy-start.12 = (f32[1,2,2,64,64]{3,2,4,1,0:T(2,128)S(1)}, f32[1,2,2,64,64]{3,2,4,1,0:T(2,128)}, u32[]{:S(2)}) copy-start(f32[1,2,2,64,64]{3,2,4,1,0:T(2,128)} %stack.152) | copy-start | bytes 196612
  175.9 6.7 %copy-start.13 = (f32[1,2,2,64,64]{3,2,4,1,0:T(2,128)S(1)}, f32[1,2,2,64,64]{3,2,4,1,0:T(2,128)}, u32[]{:S(2)}) copy-start(f32[1,2,2,64,64]{3,2,4,1,0:T(2,128)} %stack.155) | copy-start | bytes 196612
  182.9 47.3 %copy-start.23 = (f32[128,2]{0,1:T(2,128)S(1)}, f32[128,2]{0,1:T(2,128)}, u32[]{:S(2)}) copy-start(f32[128,2]{0,1:T(2,128)} %param.41) | copy-start | bytes 3076
  183.0 47.3 %copy-start.31 = (f32[128]{0:T(128)S(1)}, f32[128]{0:T(128)}, u32[]{:S(2)}) copy-start(f32[128]{0:T(128)} %copy-done.30) | copy-start | bytes 1540
  231.2 2.3 copy-start.27
  233.1 3.5 copy-start.7
  238.3 1.1 copy-start.19
  238.5 0.6 copy-start.9
  238.5 1.4 copy-start.18
  284.5 83.1 %all-to-all-start.2 = ((bf16[16,256,64]{1,2,0:T(8,128)(2,1)}), bf16[16,256,64]{1,2,0:T(8,128)(2,1)S(1)}, u32[]{:S(2)}, u32[]{:S(2)}) async-start(bf16[16,256,64]{1,2,0:T(8,128)(2,1)} %broadcast_in_dim.44), calls=%async_computation.2 | async-start | bytes 1048576 | tf_op jit(solution)/shard_map/all_to_all | solution.py:16
  342.6 2.3 copy-start.17
  344.9 18.1 %copy-start.10 = (f32[2,128,64]{1,2,0:T(8,128)S(1)}, f32[2,128,64]{1,2,0:T(8,128)}, u32[]{:S(2)}) copy-start(f32[2,128,64]{1,2,0:T(8,128)} %copy-done.9) | copy-start | bytes 196612
  367.6 2.4 copy-start.22
  370.1 1.7 copy-start.4
  370.2 1.9 copy-start.15
  372.3 1.0 copy-start.11
  372.3 1.1 copy-start.20
  373.4 1.1 copy-start.21
  423.0 1.8 copy-start.24
  423.0 1.9 copy-start.2
  425.3 40.3 %copy-start.6 = (bf16[8,4096]{1,0:T(8,128)(2,1)S(1)}, bf16[8,4096]{1,0:T(8,128)(2,1)}, u32[]{:S(2)}) copy-start(bf16[8,4096]{1,0:T(8,128)(2,1)} %param.27) | copy-start | bytes 196612
Sparse Core Ops, SparseCore 0:
  176.8 53.3 all-gather.2
